TPU v7x, 32 devices: a whole 2x2x4 slice. The times are simulated.
32 devices in a mesh: sp: 8 (over z, y), tp: 4 (over x, core).
Axes of the slice: x: 2, y: 2, z: 4, core: 2. Of those that a mesh axis runs over, the one named last changes fastest.
Arguments:
- residual: bfloat16 [6144, 2048], P(('sp', 'tp')), may hold values from -6 to 6
- queries: bfloat16 [6144, 1024], P('sp', 'tp'), may hold values from -240 to 240
- keys: bfloat16 [6144, 256], P('sp', 'tp'), may hold values from -6 to 6
- values: bfloat16 [6144, 256], P('sp', 'tp'), may hold values from -18 to 18
- sinks: float32 [16], P('tp'), may hold values from 1 to 6
- out_weight: bfloat16 [1024, 2048], replicated, may hold values from -0.5625 to 0.5625
- norm_gain: float32 [2048], replicated, may hold values from 0.1 to 1.9
- gate_weight: bfloat16 [2048, 5632], P('sp', 'tp'), may hold values from -0.125 to 0.125
- up_weight: bfloat16 [2048, 5632], P('sp', 'tp'), may hold values from -0.125 to 0.125
- down_weight: bfloat16 [5632, 2048], P('tp', 'sp'), may hold values from -0.078125 to 0.078125
Outputs:
- layer_out: bfloat16 [6144, 2048], P(('sp', 'tp'))
All inputs are finite; a program needn't handle non-finite values.
Results may differ from a plain program's by a relative error of at most 0.014.
Values may be sent and summed in bfloat16 or wider, within the bound.
No kernel may reach another device: no remote copies, remote signals or barrier semaphores. Data moves between devices by JAX's collectives and lax.ppermute only.
A program may use at most 128 MiB of HBM per device.

v0:
```python
import jax
import jax.numpy as jnp
from jax import lax
from jax.sharding import PartitionSpec as P

HEAD = 64
WINDOW = 128


def passed_along(block, axis, distance):
    devices = range(lax.axis_size(axis))
    route = [(i - distance, i) for i in devices if i - distance in devices]
    return lax.ppermute(block, axis, route)


def attend(queries, keys_ext, values_ext, sinks, block_base):
    rows = queries.shape[0]
    nblk = rows // WINDOW
    qheads = sinks.shape[0]
    kheads = keys_ext.shape[1] // HEAD
    group = qheads // kheads
    qblock = queries.reshape(nblk, WINDOW, kheads, group, HEAD).astype(jnp.float32)

    def band(arr):
        first = arr[:rows].reshape(nblk, WINDOW, kheads, HEAD)
        second = arr[WINDOW:].reshape(nblk, WINDOW, kheads, HEAD)
        return jnp.concatenate([first, second], axis=1).astype(jnp.float32)

    kband = band(keys_ext)
    vband = band(values_ext)
    score = jnp.einsum("nqhgd,nkhd->nhgqk", qblock, kband) * HEAD ** (-0.5)
    qidx = jnp.arange(WINDOW)[:, None]
    kidx = jnp.arange(2 * WINDOW)[None, :]
    rel = qidx + WINDOW - kidx
    valid = (rel >= 0) & (rel < WINDOW)
    blocks = block_base + jnp.arange(nblk)
    valid = valid[None] & ((blocks > 0)[:, None, None] | (kidx >= WINDOW)[None])
    score = jnp.where(valid[:, None, None], score, -jnp.inf)
    sink = sinks.reshape(kheads, group)[None, :, :, None]
    top = jnp.maximum(jnp.max(score, axis=-1), sink)
    expd = jnp.exp(score - top[..., None])
    denom = jnp.sum(expd, axis=-1) + jnp.exp(sink - top)
    weights = (expd / denom[..., None]).astype(jnp.bfloat16)
    result = jnp.einsum("nhgqk,nkhd->nqhgd", weights.astype(jnp.float32), vband)
    return result.reshape(rows, qheads * HEAD).astype(jnp.bfloat16)


def shards(
    residual,
    queries,
    keys,
    values,
    sinks,
    out_weight,
    norm_gain,
    gate_weight,
    up_weight,
    down_weight,
):
    rows_dev = queries.shape[0]
    prev_keys, prev_values = passed_along((keys[-WINDOW:], values[-WINDOW:]), "sp", 1)
    keys_ext = jnp.concatenate([prev_keys, keys], axis=0)
    values_ext = jnp.concatenate([prev_values, values], axis=0)
    attention = attend(
        queries, keys_ext, values_ext, sinks, lax.axis_index("sp") * (rows_dev // WINDOW)
    )
    width = attention.shape[1]
    mine = lax.dynamic_slice_in_dim(out_weight, lax.axis_index("tp") * width, width, 0)
    proj = lax.psum_scatter(
        jnp.dot(attention, mine, preferred_element_type=jnp.float32).astype(jnp.bfloat16),
        "tp",
        scatter_dimension=0,
        tiled=True,
    ).astype(jnp.float32)
    mixed = (residual.astype(jnp.float32) + proj).astype(jnp.bfloat16)
    mixf = mixed.astype(jnp.float32)
    normed = (
        mixf * lax.rsqrt(jnp.mean(mixf * mixf, axis=-1, keepdims=True) + 1e-06) * norm_gain
    ).astype(jnp.bfloat16)
    normed_all = lax.all_gather(normed, "tp", axis=0, tiled=True)
    gate = jnp.dot(
        normed_all,
        lax.all_gather(gate_weight, "sp", axis=0, tiled=True),
        preferred_element_type=jnp.float32,
    )
    upper = jnp.dot(
        normed_all,
        lax.all_gather(up_weight, "sp", axis=0, tiled=True),
        preferred_element_type=jnp.float32,
    )
    hidden = (jax.nn.silu(gate) * upper).astype(jnp.bfloat16)
    terms = jnp.dot(
        hidden,
        lax.all_gather(down_weight, "sp", axis=1, tiled=True),
        preferred_element_type=jnp.float32,
    )
    ffn = lax.psum_scatter(
        terms.astype(jnp.bfloat16), "tp", scatter_dimension=0, tiled=True
    ).astype(jnp.float32)
    return (mixed.astype(jnp.float32) + ffn).astype(jnp.bfloat16)


def solution(mesh):
    placed = (
        P(("sp", "tp"), None),
        P("sp", "tp"),
        P("sp", "tp"),
        P("sp", "tp"),
        P("tp"),
        P(),
        P(),
        P("sp", "tp"),
        P("sp", "tp"),
        P("tp", "sp"),
    )
    return jax.shard_map(
        shards, mesh=mesh, in_specs=placed, out_specs=P(("sp", "tp"), None), check_vma=False
    )
```

profile of v0, /device:TPU:0, one launch (start us, length us, event | category | flops | bytes accessed | tf_op | source)
XLA Modules:
  0.0 407.9 jit_solution(3157988359120101178)
XLA Ops:
  7.4 0.0 reduce-scatter.3.cloned.1.call-start
  7.4 0.7 slice.14
  8.1 4.9 %collective-permute-start.1 = (bf16[128,64]{0,1:T(8,128)(2,1)S(1)}, bf16[128,64]{0,1:T(8,128)(2,1)S(1)}, u32[]{:S(2)}, u32[]{:S(2)}) collective-permute-start(bf16[128,64]{0,1:T(8,128)(2,1)S(1)} %slice.14), channel_id=1, source_target_pairs={{0,4},{4,8},{8,12},{12,16},{16,20},{20,24},{24,28},{1,5},{5,9},{9,... | collective-permute-start | bytes 49160 | tf_op jit(solution)/shard_map/ppermute | solution.py:13
  13.0 0.7 slice.12
  13.7 3.4 collective-permute-start
  17.2 0.1 broadcast_or_fusion
  17.3 0.3 broadcast_and_fusion
  17.6 1.0 reshape.145
  18.6 1.0 reshape.142
  19.6 0.0 copy-start.4
  19.6 2.5 reshape.151
  22.2 0.6 copy.14
  22.9 0.0 collective-permute-done.1
  22.9 0.9 pad_maximum_fusion
  23.8 0.1 reshape.144
  23.9 0.0 copy-start.2
  23.9 1.9 fusion.1
  25.8 0.0 copy-done.4
  25.8 0.1 broadcast_maximum_fusion
  25.9 0.7 fusion
  26.6 0.1 exponential_add_fusion
  26.7 0.0 collective-permute-done
  26.7 0.0 copy-done.2
  26.7 0.7 pad_maximum_fusion.1
  27.3 1.0 reshape.141
  28.4 1.8 fusion.12
  30.2 0.3 copy.20
  30.5 4.0 convolution_convert_fusion
  34.5 0.0 copy-start
  34.5 0.0 copy-start.3
  34.5 0.0 reduce-scatter.3.cloned.1.call-update
  34.5 0.0 all-gather.7.cloned.1.call-start
  34.6 0.5 all-gather.7.cloned.1.call-update
  35.1 0.0 all-gather.5.cloned.1.call-start
  35.1 37.7 %reduce-scatter.3.cloned.1.call-done = bf16[192,2048]{1,0:T(8,128)(2,1)} async-done(((bf16[768,2048]{1,0:T(8,128)(2,1)}), bf16[192,2048]{1,0:T(8,128)(2,1)}) %reduce-scatter.3.cloned.1.call-update) | async-done | bytes 786448 | tf_op jit(solution)/shard_map/reduce_scatter | solution.py:69
  72.8 0.0 copy-done
  72.8 1.5 fusion.2
  74.3 0.0 copy-done.3
  74.3 2.3 fusion.4
  76.6 0.0 all-gather.5.cloned.1.call-update
  76.6 0.0 all-gather.11.cloned.1.call-start
  76.7 0.5 all-gather.11.cloned.1.call-update
  77.2 0.0 all-gather.9.cloned.1.call-start
  77.3 0.7 all-gather.9.cloned.1.call-update
  77.9 0.2 reduce-scatter.5.cloned.1.call-start
  78.2 51.4 %all-gather.7.cloned.1.call-done = bf16[2048,1408]{1,0:T(8,128)(2,1)} async-done(((bf16[256,1408]{1,0:T(8,128)(2,1)}), bf16[2048,1408]{1,0:T(8,128)(2,1)}) %all-gather.7.cloned.1.call-update) | async-done | bytes 5767184 | tf_op jit(solution)/shard_map/all_gather | solution.py:83
  129.6 28.0 %all-gather.5.cloned.1.call-done = bf16[768,2048]{1,0:T(8,128)(2,1)} async-done(((bf16[192,2048]{1,0:T(8,128)(2,1)}), bf16[768,2048]{1,0:T(8,128)(2,1)}) %all-gather.5.cloned.1.call-update) | async-done | bytes 3145744 | tf_op jit(solution)/shard_map/all_gather | solution.py:80
  157.6 9.7 %fusion.33 = f32[768,1408]{1,0:T(8,128)} fusion(bf16[768,2048]{1,0:T(8,128)(2,1)} %all-gather.5.cloned.1.call-done, bf16[2048,1408]{1,0:T(8,128)(2,1)} %all-gather.7.cloned.1.call-done), kind=kOutput, calls=%fused_computation.52 | convolution fusion | flops 4429185024 | bytes 13238272 | tf_op jit(solution)/shard_map/dot_general | solution.py:81
  167.2 85.1 %all-gather.11.cloned.1.call-done = bf16[1408,2048]{1,0:T(8,128)(2,1)} async-done(((bf16[1408,256]{1,0:T(8,128)(2,1)}), bf16[1408,2048]{1,0:T(8,128)(2,1)}) %all-gather.11.cloned.1.call-update) | async-done | bytes 5767184 | tf_op jit(solution)/shard_map/all_gather | solution.py:94
  252.4 92.5 %all-gather.9.cloned.1.call-done = bf16[2048,1408]{1,0:T(8,128)(2,1)} async-done(((bf16[256,1408]{1,0:T(8,128)(2,1)}), bf16[2048,1408]{1,0:T(8,128)(2,1)}) %all-gather.9.cloned.1.call-update) | async-done | bytes 5767184 | tf_op jit(solution)/shard_map/all_gather | solution.py:88
  344.9 16.8 %convolution_convert_fusion.1 = bf16[768,2048]{1,0:T(8,128)(2,1)} fusion(bf16[1408,2048]{1,0:T(8,128)(2,1)} %all-gather.11.cloned.1.call-done, f32[768,1408]{1,0:T(8,128)} %fusion.33, bf16[768,2048]{1,0:T(8,128)(2,1)} %all-gather.5.cloned.1.call-done, bf16[2048,1408]{1,0:T(8,128)(2,1)} %all-gather.9.cloned.1.call-done), kind=kOutput, calls=%fused_computation.2 | convolution fusion | flops 8866430976 | bytes 22151168 | tf_op jit(solution)/shard_map/dot_general | solution.py:92
  361.7 0.0 copy-start.1
  361.7 0.0 reduce-scatter.5.cloned.1.call-update
  361.7 36.2 %reduce-scatter.5.cloned.1.call-done = bf16[192,2048]{1,0:T(8,128)(2,1)} async-done(((bf16[768,2048]{1,0:T(8,128)(2,1)}), bf16[192,2048]{1,0:T(8,128)(2,1)}) %reduce-scatter.5.cloned.1.call-update) | async-done | bytes 786448 | tf_op jit(solution)/shard_map/reduce_scatter | solution.py:97
  397.9 0.0 copy-done.1
  397.9 2.4 fusion.5
  (8 shorter events, 0.1 us)
Async XLA Ops:
  7.4 65.4 %reduce-scatter.3.cloned.1.call-start = ((), (), s32[]{:S(2)}) async-start(), calls=%async_computation.2 | async-start | bytes 3932160 | tf_op jit(solution)/shard_map/reduce_scatter | solution.py:69
  8.1 14.8 %collective-permute-start.1 = (bf16[128,64]{0,1:T(8,128)(2,1)S(1)}, bf16[128,64]{0,1:T(8,128)(2,1)S(1)}, u32[]{:S(2)}, u32[]{:S(2)}) collective-permute-start(bf16[128,64]{0,1:T(8,128)(2,1)S(1)} %slice.14), channel_id=1, source_target_pairs={{0,4},{4,8},{8,12},{12,16},{16,20},{20,24},{24,28},{1,5},{5,9},{9,... | collective-permute-start | bytes 49160 | tf_op jit(solution)/shard_map/ppermute | solution.py:13
  13.7 13.0 %collective-permute-start = (bf16[128,64]{0,1:T(8,128)(2,1)S(1)}, bf16[128,64]{0,1:T(8,128)(2,1)S(1)}, u32[]{:S(2)}, u32[]{:S(2)}) collective-permute-start(bf16[128,64]{0,1:T(8,128)(2,1)S(1)} %slice.12), channel_id=1, source_target_pairs={{0,4},{4,8},{8,12},{12,16},{16,20},{20,24},{24,28},{1,5},{5,9},{9,... | collective-permute-start | bytes 49160 | tf_op jit(solution)/shard_map/ppermute | solution.py:13
  19.6 6.2 %copy-start.4 = (f32[4]{0:T(128)S(1)}, f32[4]{0:T(128)}, u32[]{:S(2)}) copy-start(f32[4]{0:T(128)} %param.14) | copy-start | bytes 52
  23.9 2.8 copy-start.2
  34.5 38.3 %copy-start = (bf16[192,2048]{1,0:T(8,128)(2,1)S(1)}, bf16[192,2048]{1,0:T(8,128)(2,1)}, u32[]{:S(2)}) copy-start(bf16[192,2048]{1,0:T(8,128)(2,1)} %param.10) | copy-start | bytes 2359300
  34.5 39.8 %copy-start.3 = (f32[2048]{0:T(1024)S(1)}, f32[2048]{0:T(1024)}, u32[]{:S(2)}) copy-start(f32[2048]{0:T(1024)} %param.16) | copy-start | bytes 24580
  34.5 95.1 %all-gather.7.cloned.1.call-start = ((), (), s32[]{:S(2)}) async-start(), calls=%async_computation.4 | async-start | bytes 6488064 | tf_op jit(solution)/shard_map/all_gather | solution.py:83
  35.1 122.5 %all-gather.5.cloned.1.call-start = ((), (), s32[]{:S(2)}) async-start(), calls=%async_computation.3 | async-start | bytes 3932160 | tf_op jit(solution)/shard_map/all_gather | solution.py:80
  76.6 175.8 %all-gather.11.cloned.1.call-start = ((), (), s32[]{:S(2)}) async-start(), calls=%async_computation.6 | async-start | bytes 6488064 | tf_op jit(solution)/shard_map/all_gather | solution.py:94
  77.2 267.7 %all-gather.9.cloned.1.call-start = ((), (), s32[]{:S(2)}) async-start(), calls=%async_computation.5 | async-start | bytes 6488064 | tf_op jit(solution)/shard_map/all_gather | solution.py:88
  77.9 320.0 %reduce-scatter.5.cloned.1.call-start = ((), (), s32[]{:S(2)}) async-start(), calls=%async_computation.7 | async-start | bytes 3932160 | tf_op jit(solution)/shard_map/reduce_scatter | solution.py:97
  361.7 36.2 %copy-start.1 = (bf16[192,2048]{1,0:T(8,128)(2,1)S(1)}, bf16[192,2048]{1,0:T(8,128)(2,1)}, u32[]{:S(2)}) copy-start(bf16[192,2048]{1,0:T(8,128)(2,1)} %reduce-scatter.3.cloned.1.call-done) | copy-start | bytes 2359300
Sparse Core Ops, SparseCore 0:
  34.6 38.1 reduce-scatter.2
  361.9 35.9 reduce-scatter.4
Sparse Core Ops, SparseCore 1:
  37.2 92.4 all-gather.6
  131.0 26.5 all-gather.4
  159.5 92.9 all-gather.10
  254.6 90.3 all-gather.8
where the time goes:
time: 409 us; the launch traced here: 408 us
  waiting for transfers between devices  333 us (81%)
  matrix products  34.1 us (8%)
  between operations  15.2 us (4%)
  other arithmetic  8.99 us (2%)
  starting transfers between devices  8.7 us (2%)
  local copies, waits for them, and re-layouts  8.18 us (2%)
    all_gather x1, waiting for transfers between devices, shards(): lax.all_gather(up_weight, 'sp', axis=0, tiled=True)  92.5 us
    all_gather x1, waiting for transfers between devices, shards(): lax.all_gather(down_weight, 'sp', axis=1, tiled=True)  85.1 us
    all_gather x1, waiting for transfers between devices, shards(): lax.all_gather(gate_weight, 'sp', axis=0, tiled=True)  51.4 us
    reduce_scatter x1, waiting for transfers between devices, shards(): lax.psum_scatter(jnp.dot(attention, mine, preferred_element_type=jnp.floa...  37.7 us
    reduce_scatter x1, waiting for transfers between devices, shards(): lax.psum_scatter(terms.astype(jnp.bfloat16), 'tp', scatter_dimension=0, t...  36.2 us
    all_gather x1, waiting for transfers between devices, shards(): normed_all = lax.all_gather(normed, 'tp', axis=0, tiled=True)  28 us
    dot_general x1, matrix products, shards(): jnp.dot(hidden, lax.all_gather(down_weight, 'sp', axis=1, tiled=True), pr...  16.8 us
    dot_general x1, matrix products, shards(): jnp.dot(normed_all, lax.all_gather(gate_weight, 'sp', axis=0, tiled=True)...  9.69 us
  transfers between devices with their start and end apart: 8, of which 6 were waited for; matrix products, arithmetic and copies ran while one was open for 6% of the time, Pallas kernels for 0%

commit v1 on v0

--- a/solution.py
+++ b/solution.py
@@ -5,6 +5,17 @@
 
 HEAD = 64
 WINDOW = 128
+
+
+def around_the_ring(block, axis, along):
+    peers = lax.axis_size(axis)
+    right = [(i, (i + 1) % peers) for i in range(peers)]
+    parts = [block]
+    for stride in range(1, peers):
+        parts = [lax.ppermute(parts[0], axis, right), *parts]
+    whole = jnp.concatenate(parts, axis=along)
+    shift = (lax.axis_index(axis) + 1) * parts[-1].shape[along]
+    return jnp.roll(whole, shift, axis=along)
 
 
 def passed_along(block, axis, distance):
@@ -77,7 +88,7 @@
     normed = (
         mixf * lax.rsqrt(jnp.mean(mixf * mixf, axis=-1, keepdims=True) + 1e-06) * norm_gain
     ).astype(jnp.bfloat16)
-    normed_all = lax.all_gather(normed, "tp", axis=0, tiled=True)
+    normed_all = around_the_ring(normed, "tp", 0)
     gate = jnp.dot(
         normed_all,
         lax.all_gather(gate_weight, "sp", axis=0, tiled=True),

time: 409 us -> 377 us (0.922)
  waiting for transfers between devices: 333 us -> 294 us
  local copies, waits for them, and re-layouts: 8.18 us -> 17.4 us
    all_gather x1, waiting for transfers between devices: 51.4 us -> 9.53 us  [shards(): lax.all_gather(gate_weight, 'sp', axis=0, tiled=True)]
    ppermute x0 -> x3, waiting for transfers between devices: none -> 34.3 us  [around_the_ring(): parts = [lax.ppermute(parts[0], axis, right), *parts]]
    all_gather x1 -> x0, waiting for transfers between devices: 28 us -> none  [shards(): normed_all = lax.all_gather(normed, 'tp', axis=0, tiled=True)]
    unnamed x10 -> x19, local copies, waits for them, and re-layouts: 0.02 us -> 10.5 us
    all_gather x1, waiting for transfers between devices: 92.5 us -> 82.7 us  [shards(): lax.all_gather(up_weight, 'sp', axis=0, tiled=True)]
    all_gather x1, waiting for transfers between devices: 85.1 us -> 93 us  [shards(): lax.all_gather(down_weight, 'sp', axis=1, tiled=True)]
  transfers between devices with their start and end apart: 8 -> 10, of which waited for: 6 -> 8; matrix products, arithmetic and copies ran while one was open for 6% -> 8% of each run, Pallas kernels for 0% -> 0%
where the time goes in v1:
time: 377 us
  waiting for transfers between devices  294 us (78%)
  matrix products  34 us (9%)
  local copies, waits for them, and re-layouts  17.4 us (5%)
  between operations  15.3 us (4%)
  starting transfers between devices  8.53 us (2%)
  other arithmetic  7.54 us (2%)
    all_gather x1, waiting for transfers between devices, shards(): lax.all_gather(down_weight, 'sp', axis=1, tiled=True)  93 us
    all_gather x1, waiting for transfers between devices, shards(): lax.all_gather(up_weight, 'sp', axis=0, tiled=True)  82.7 us
    reduce_scatter x1, waiting for transfers between devices, shards(): lax.psum_scatter(jnp.dot(attention, mine, preferred_element_type=jnp.floa...  36.5 us
    reduce_scatter x1, waiting for transfers between devices, shards(): lax.psum_scatter(terms.astype(jnp.bfloat16), 'tp', scatter_dimension=0, t...  36.2 us
    ppermute x3, waiting for transfers between devices, around_the_ring(): parts = [lax.ppermute(parts[0], axis, right), *parts]  34.3 us
    dot_general x1, matrix products, shards(): jnp.dot(hidden, lax.all_gather(down_weight, 'sp', axis=1, tiled=True), pr...  16.8 us
    unnamed x19, local copies, waits for them, and re-layouts  10.5 us
    dot_general x1, matrix products, shards(): jnp.dot(normed_all, lax.all_gather(gate_weight, 'sp', axis=0, tiled=True)...  9.7 us
  transfers between devices with their start and end apart: 10, of which 8 were waited for; matrix products, arithmetic and copies ran while one was open for 8% of the time, Pallas kernels for 0%

profile of v1, /device:TPU:0, one launch (start us, length us, event | category | flops | bytes accessed | tf_op | source)
XLA Modules:
  0.0 376.5 jit_solution(2537932385554947819)
XLA Ops:
  7.4 0.0 reduce-scatter.3.cloned.1.call-start
  7.4 0.7 slice.14
  8.1 4.9 %collective-permute-start.1 = (bf16[128,64]{0,1:T(8,128)(2,1)S(1)}, bf16[128,64]{0,1:T(8,128)(2,1)S(1)}, u32[]{:S(2)}, u32[]{:S(2)}) collective-permute-start(bf16[128,64]{0,1:T(8,128)(2,1)S(1)} %slice.14), channel_id=1, source_target_pairs={{0,4},{4,8},{8,12},{12,16},{16,20},{20,24},{24,28},{1,5},{5,9},{9,... | collective-permute-start | bytes 49160 | tf_op jit(solution)/shard_map/ppermute | solution.py:24
  13.0 0.7 slice.12
  13.7 3.4 collective-permute-start
  17.2 0.1 broadcast_or_fusion
  17.3 0.3 broadcast_and_fusion
  17.6 1.0 reshape.145
  18.6 1.0 reshape.142
  19.6 1.8 reshape.151
  21.5 0.0 collective-permute-done.1
  21.6 0.9 pad_maximum_fusion
  22.5 0.0 copy-start.3
  22.5 0.1 reshape.144
  22.6 0.7 fusion.7
  23.4 0.0 copy-start.2
  23.4 0.0 copy-done.5
  23.4 0.1 broadcast_maximum_fusion
  23.5 1.5 copy-done.2
  25.0 0.7 fusion
  25.7 0.1 exponential_add_fusion
  25.8 0.0 collective-permute-done
  25.8 0.0 copy-done.3
  25.8 0.1 reshape.141
  26.0 2.8 fusion.18
  28.8 0.3 copy.20
  29.1 0.0 copy-start
  29.1 4.0 %convolution_convert_fusion = bf16[768,2048]{1,0:T(8,128)(2,1)} fusion(bf16[1024,2048]{1,0:T(8,128)(2,1)} %param.15, s32[]{:T(128)S(6)} %select_n.21, bf16[32,8,6,128]{3,2,1,0:T(8,128)(2,1)S(1)} %bitcast.60), kind=kOutput, calls=%fused_computation.1 | convolution fusion | flops 806879232 | bytes 4587524 | tf_op jit(solution)/shard_map/dot_general | solution.py:81
  33.1 0.0 reduce-scatter.3.cloned.1.call-update
  33.1 0.0 all-gather.4.cloned.1.call-start
  33.2 0.5 all-gather.4.cloned.1.call-update
  33.7 0.0 all-gather.6.cloned.1.call-start
  33.7 0.5 all-gather.6.cloned.1.call-update
  34.3 0.0 all-gather.8.cloned.1.call-start
  34.3 0.5 all-gather.8.cloned.1.call-update
  34.9 0.0 reduce-scatter.5.cloned.1.call-start
  34.9 36.5 %reduce-scatter.3.cloned.1.call-done = bf16[192,2048]{1,0:T(8,128)(2,1)} async-done(((bf16[768,2048]{1,0:T(8,128)(2,1)}), bf16[192,2048]{1,0:T(8,128)(2,1)}) %reduce-scatter.3.cloned.1.call-update) | async-done | bytes 786448 | tf_op jit(solution)/shard_map/reduce_scatter | solution.py:80
  71.4 0.0 copy-done
  71.4 1.5 fusion.8
  72.9 0.0 copy-done.4
  72.9 1.5 fusion.10
  74.3 0.1 collective-permute-start.2
  74.4 11.4 %collective-permute-done.2 = bf16[192,2048]{1,0:T(8,128)(2,1)S(1)} collective-permute-done((bf16[192,2048]{1,0:T(8,128)(2,1)S(1)}, bf16[192,2048]{1,0:T(8,128)(2,1)S(1)}, u32[]{:S(2)}, u32[]{:S(2)}) %collective-permute-start.2) | collective-permute-done | bytes 786464 | tf_op jit(solution)/shard_map/ppermute | solution.py:15
  85.8 0.0 collective-permute-start.3
  85.8 11.4 %collective-permute-done.3 = bf16[192,2048]{1,0:T(8,128)(2,1)S(1)} collective-permute-done((bf16[192,2048]{1,0:T(8,128)(2,1)S(1)}, bf16[192,2048]{1,0:T(8,128)(2,1)S(1)}, u32[]{:S(2)}, u32[]{:S(2)}) %collective-permute-start.3) | collective-permute-done | bytes 786464 | tf_op jit(solution)/shard_map/ppermute | solution.py:15
  97.2 0.0 collective-permute-start.4
  97.2 11.5 %collective-permute-done.4 = bf16[192,2048]{1,0:T(8,128)(2,1)} collective-permute-done((bf16[192,2048]{1,0:T(8,128)(2,1)S(1)}, bf16[192,2048]{1,0:T(8,128)(2,1)}, u32[]{:S(2)}, u32[]{:S(2)}) %collective-permute-start.4) | collective-permute-done | bytes 786464 | tf_op jit(solution)/shard_map/ppermute | solution.py:15
  108.7 2.1 constant_dynamic-update-slice_fusion.7
  110.8 1.0 constant_dynamic-update-slice_fusion.6
  111.8 0.9 constant_dynamic-update-slice_fusion.5
  112.7 0.9 constant_dynamic-update-slice_fusion.4
  113.7 2.1 constant_dynamic-update-slice_fusion.3
  115.8 0.9 constant_dynamic-update-slice_fusion.2
  116.7 1.0 constant_dynamic-update-slice_fusion.1
  117.7 0.9 constant_dynamic-update-slice_fusion
  118.6 9.5 %all-gather.4.cloned.1.call-done = bf16[2048,1408]{1,0:T(8,128)(2,1)} async-done(((bf16[256,1408]{1,0:T(8,128)(2,1)}), bf16[2048,1408]{1,0:T(8,128)(2,1)}) %all-gather.4.cloned.1.call-update) | async-done | bytes 5767184 | tf_op jit(solution)/shard_map/all_gather | solution.py:94
  128.2 9.7 %fusion.3 = f32[768,1408]{1,0:T(8,128)} fusion(bf16[2048,1408]{1,0:T(8,128)(2,1)} %all-gather.4.cloned.1.call-done, bf16[1536,2048]{1,0:T(8,128)(2,1)} %constant_dynamic-update-slice_fusion, s32[]{:T(128)S(6)} %select_n.23), kind=kOutput, calls=%fused_computation.9 | convolution fusion | flops 4429185024 | bytes 13238276 | tf_op jit(solution)/shard_map/dot_general | solution.py:92
  137.9 82.7 %all-gather.6.cloned.1.call-done = bf16[2048,1408]{1,0:T(8,128)(2,1)} async-done(((bf16[256,1408]{1,0:T(8,128)(2,1)}), bf16[2048,1408]{1,0:T(8,128)(2,1)}) %all-gather.6.cloned.1.call-update) | async-done | bytes 5767184 | tf_op jit(solution)/shard_map/all_gather | solution.py:99
  220.5 93.0 %all-gather.8.cloned.1.call-done = bf16[1408,2048]{1,0:T(8,128)(2,1)} async-done(((bf16[1408,256]{1,0:T(8,128)(2,1)}), bf16[1408,2048]{1,0:T(8,128)(2,1)}) %all-gather.8.cloned.1.call-update) | async-done | bytes 5767184 | tf_op jit(solution)/shard_map/all_gather | solution.py:105
  313.5 16.8 %convolution_convert_fusion.1 = bf16[768,2048]{1,0:T(8,128)(2,1)} fusion(bf16[1408,2048]{1,0:T(8,128)(2,1)} %all-gather.8.cloned.1.call-done, f32[768,1408]{1,0:T(8,128)} %fusion.3, bf16[2048,1408]{1,0:T(8,128)(2,1)} %all-gather.6.cloned.1.call-done, bf16[1536,2048]{1,0:T(8,128)(2,1)} %constant_dynamic-update-slice_fusion, s32[]{:T(128)S(6)} %select_n.23), kind=kOutput, calls=%fused_computation.2 | convolution fusion | flops 8866430976 | bytes 22151172 | tf_op jit(solution)/shard_map/dot_general | solution.py:103
  330.3 0.0 reduce-scatter.5.cloned.1.call-update
  330.3 36.2 %reduce-scatter.5.cloned.1.call-done = bf16[192,2048]{1,0:T(8,128)(2,1)} async-done(((bf16[768,2048]{1,0:T(8,128)(2,1)}), bf16[192,2048]{1,0:T(8,128)(2,1)}) %reduce-scatter.5.cloned.1.call-update) | async-done | bytes 786448 | tf_op jit(solution)/shard_map/reduce_scatter | solution.py:108
  366.5 0.0 copy-done.1
  366.5 2.4 fusion.11
  (13 shorter events, 0.1 us)
Async XLA Ops:
  7.4 16.0 %copy-start.5 = (f32[4]{0:T(128)S(1)}, f32[4]{0:T(128)}, u32[]{:S(2)}) copy-start(f32[4]{0:T(128)} %param.14) | copy-start | bytes 52
  7.4 64.0 %reduce-scatter.3.cloned.1.call-start = ((), (), s32[]{:S(2)}) async-start(), calls=%async_computation.2 | async-start | bytes 3932160 | tf_op jit(solution)/shard_map/reduce_scatter | solution.py:80
  8.1 13.4 %collective-permute-start.1 = (bf16[128,64]{0,1:T(8,128)(2,1)S(1)}, bf16[128,64]{0,1:T(8,128)(2,1)S(1)}, u32[]{:S(2)}, u32[]{:S(2)}) collective-permute-start(bf16[128,64]{0,1:T(8,128)(2,1)S(1)} %slice.14), channel_id=1, source_target_pairs={{0,4},{4,8},{8,12},{12,16},{16,20},{20,24},{24,28},{1,5},{5,9},{9,... | collective-permute-start | bytes 49160 | tf_op jit(solution)/shard_map/ppermute | solution.py:24
  13.7 12.1 %collective-permute-start = (bf16[128,64]{0,1:T(8,128)(2,1)S(1)}, bf16[128,64]{0,1:T(8,128)(2,1)S(1)}, u32[]{:S(2)}, u32[]{:S(2)}) collective-permute-start(bf16[128,64]{0,1:T(8,128)(2,1)S(1)} %slice.12), channel_id=1, source_target_pairs={{0,4},{4,8},{8,12},{12,16},{16,20},{20,24},{24,28},{1,5},{5,9},{9,... | collective-permute-start | bytes 49160 | tf_op jit(solution)/shard_map/ppermute | solution.py:24
  22.5 3.4 copy-start.3
  23.4 1.6 copy-start.2
  29.1 42.3 %copy-start = (bf16[192,2048]{1,0:T(8,128)(2,1)S(1)}, bf16[192,2048]{1,0:T(8,128)(2,1)}, u32[]{:S(2)}) copy-start(bf16[192,2048]{1,0:T(8,128)(2,1)} %param.10) | copy-start | bytes 2359300
  33.1 39.8 %copy-start.4 = (f32[2048]{0:T(1024)S(1)}, f32[2048]{0:T(1024)}, u32[]{:S(2)}) copy-start(f32[2048]{0:T(1024)} %param.16) | copy-start | bytes 24580
  33.1 95.0 %all-gather.4.cloned.1.call-start = ((), (), s32[]{:S(2)}) async-start(), calls=%async_computation.3 | async-start | bytes 6488064 | tf_op jit(solution)/shard_map/all_gather | solution.py:94
  33.7 186.8 %all-gather.6.cloned.1.call-start = ((), (), s32[]{:S(2)}) async-start(), calls=%async_computation.4 | async-start | bytes 6488064 | tf_op jit(solution)/shard_map/all_gather | solution.py:99
  34.3 279.2 %all-gather.8.cloned.1.call-start = ((), (), s32[]{:S(2)}) async-start(), calls=%async_computation.5 | async-start | bytes 6488064 | tf_op jit(solution)/shard_map/all_gather | solution.py:105
  34.9 331.7 %reduce-scatter.5.cloned.1.call-start = ((), (), s32[]{:S(2)}) async-start(), calls=%async_computation.6 | async-start | bytes 3932160 | tf_op jit(solution)/shard_map/reduce_scatter | solution.py:108
  74.3 11.5 %collective-permute-start.2 = (bf16[192,2048]{1,0:T(8,128)(2,1)S(1)}, bf16[192,2048]{1,0:T(8,128)(2,1)S(1)}, u32[]{:S(2)}, u32[]{:S(2)}) collective-permute-start(bf16[192,2048]{1,0:T(8,128)(2,1)S(1)} %fusion.10), channel_id=1, source_target_pairs={{0,1},{1,2},{2,3},{3,0},{4,5},{5,6},{6,7},{7,4},{8,9},{9,10},{10,1... | collective-permute-start | bytes 2359304 | tf_op jit(solution)/shard_map/ppermute | solution.py:15
  85.8 11.4 %collective-permute-start.3 = (bf16[192,2048]{1,0:T(8,128)(2,1)S(1)}, bf16[192,2048]{1,0:T(8,128)(2,1)S(1)}, u32[]{:S(2)}, u32[]{:S(2)}) collective-permute-start(bf16[192,2048]{1,0:T(8,128)(2,1)S(1)} %collective-permute-done.2), channel_id=1, source_target_pairs={{0,1},{1,2},{2,3},{3,0},{4,5},{5,6},{6,7},{7,4},{8,9},{9,10},{10,1... | collective-permute-start | bytes 2359304 | tf_op jit(solution)/shard_map/ppermute | solution.py:15
  97.2 11.5 %collective-permute-start.4 = (bf16[192,2048]{1,0:T(8,128)(2,1)S(1)}, bf16[192,2048]{1,0:T(8,128)(2,1)}, u32[]{:S(2)}, u32[]{:S(2)}) collective-permute-start(bf16[192,2048]{1,0:T(8,128)(2,1)S(1)} %collective-permute-done.3), channel_id=1, source_target_pairs={{0,1},{1,2},{2,3},{3,0},{4,5},{5,6},{6,7},{7,4},{8,9},{9,10},{10,1... | collective-permute-start | bytes 2359304 | tf_op jit(solution)/shard_map/ppermute | solution.py:15
  137.9 228.7 %copy-start.1 = (bf16[192,2048]{1,0:T(8,128)(2,1)S(1)}, bf16[192,2048]{1,0:T(8,128)(2,1)}, u32[]{:S(2)}) copy-start(bf16[192,2048]{1,0:T(8,128)(2,1)} %reduce-scatter.3.cloned.1.call-done) | copy-start | bytes 2359300
Sparse Core Ops, SparseCore 0:
  33.2 38.0 reduce-scatter.2
  330.4 36.0 reduce-scatter.4
Sparse Core Ops, SparseCore 1:
  35.8 92.3 all-gather.3
  130.2 90.2 all-gather.5
  222.4 91.0 all-gather.7
